TPU v7x, 32 devices: a whole 2x2x4 slice. The times are simulated.
32 devices in a mesh: sp: 4 (over x, core), tp: 8 (over z, y).
Axes of the slice: x: 2, y: 2, z: 4, core: 2. Of those that a mesh axis runs over, the one named last changes fastest.
Arguments:
- latent: bfloat16 [512, 4096], P('sp', 'tp'), may hold values from -60 to 60
- context: bfloat16 [64, 4096], P('sp', 'tp'), may hold values from -6 to 6
- conditioning: bfloat16 [4096], P('sp'), may hold values from -6 to 6
- context_prompt_vector: bfloat16 [4096], P('sp'), may hold values from -6 to 6
- shift_matrix: bfloat16 [4096, 4096], P('tp', 'sp'), may hold values from -0.09375 to 0.09375
- scale_matrix: bfloat16 [4096, 4096], P('tp', 'sp'), may hold values from -0.09375 to 0.09375
- residual_gate_matrix: bfloat16 [4096, 4096], P('tp', 'sp'), may hold values from -0.09375 to 0.09375
- query_matrix: bfloat16 [2048, 4096], P('tp'), may hold values from -0.09375 to 0.09375
- key_matrix: bfloat16 [2048, 4096], P('tp'), may hold values from -0.09375 to 0.09375
- value_matrix: bfloat16 [4096, 4096], P('tp'), may hold values from -0.09375 to 0.09375
- gate_matrix: bfloat16 [4096, 4096], P('tp'), may hold values from -0.09375 to 0.09375
- decay_down_factor: bfloat16 [2, 4096, 16], replicated, may hold values from -0.09375 to 0.09375
- decay_up_factor: bfloat16 [2, 16, 2048], replicated, may hold values from -1.5 to 1.5
- decay_key_bias: float32 [2, 2048], replicated, may hold values from -0.5 to 7
- spike_log_decay: float32 [2, 512, 16], P(None, 'sp'), may hold values from -2.8 to 0
- output_gain: float32 [4096], P('tp'), may hold values from 0.1 to 1.9
- output_matrix: bfloat16 [4096, 4096], P('tp'), may hold values from -0.375 to 0.375
Outputs:
- mixed: bfloat16 [512, 4096], P('sp', 'tp')
All inputs are finite; a program needn't handle non-finite values.
Results may differ from a plain program's by a relative error of at most 0.013.
Values may be sent and summed in bfloat16 or wider, within the bound.
A program may use at most 64 MiB of HBM per device.

v0:
```python
import jax
import jax.numpy as jnp
from jax import lax
from jax.sharding import PartitionSpec as P

D = 4096
HEADS = 16
DK = 128
DECAY_RANK = 16
BLK = 64
VGROUP = 64
epsilon = 1e-05
gate_norm = 16.0
precise = lax.Precision.HIGHEST


def for_sending(value):

    def short(part):
        return part.astype(jnp.bfloat16) if part.dtype == jnp.float32 else part

    return jax.tree.map(short, value)


def from_partner(value, axis, distance):
    return lax.ppermute(value, axis, [(i, i ^ 1 << distance) for i in range(lax.axis_size(axis))])


def carried_in(value, axis, combine, identity, reverse):
    peers, index = (lax.axis_size(axis), lax.axis_index(axis))
    everything = jax.tree.map(
        lambda part, kind: lax.all_gather(part.astype(kind), axis),
        value,
        (jnp.bfloat16, jnp.bfloat16),
    )
    start = jax.tree.map(
        lambda part, zero: jnp.broadcast_to(jnp.asarray(zero, part.dtype), part.shape),
        value,
        identity,
    )

    def turn(k, before):
        at = peers - 1 - k if reverse else k
        reached = at > index if reverse else at < index
        new = combine(
            before, jax.tree.map(lambda part, own: part[at].astype(own.dtype), everything, value)
        )
        return jax.tree.map(lambda a, b: jnp.where(reached, a, b), new, before)

    return lax.fori_loop(0, peers, turn, start)


def linear(rows, weight):
    return lax.dot_general(
        rows, weight, (((1,), (1,)), ((), ())), preferred_element_type=jnp.float32
    )


def modulated(rows, row_sum, row_squares, shift_vec, scale_vec):
    rows_f = rows.astype(jnp.float32)
    mean_val = row_sum / D
    variance = row_squares / D - mean_val * mean_val
    return (
        (rows_f - mean_val) * lax.rsqrt(variance + epsilon) * (1.0 + scale_vec) + shift_vec
    ).astype(jnp.bfloat16)


def reverse_rows(array):
    return jnp.flip(array, axis=0)


def end_state(key_rows, value_rows, log_decay):
    cumulative = jnp.cumsum(log_decay, axis=0)
    totals = cumulative[-1]
    weighted = key_rows * jnp.exp(totals - cumulative)
    return (jnp.exp(totals), jnp.einsum("nhd,nhe->hde", weighted, value_rows, precision=precise))


def combine(earlier, later):
    return (earlier[0] * later[0], later[0][..., None] * earlier[1] + later[1])


def blockwise(queries, key_rows, value_rows, log_decay, carried, block_len):
    length, head_count, _ = queries.shape
    value_width = value_rows.shape[-1]
    blocks = length // block_len

    def shaped(array):
        return array.reshape(blocks, block_len, head_count, array.shape[-1])

    triangle = jnp.tril(jnp.ones((block_len, block_len), jnp.float32))

    def advance(state_now, inputs):
        block_q, block_k, block_v, block_a = inputs
        cumulative = jnp.cumsum(block_a, axis=0)
        block_end = cumulative[-1]
        query_dec = block_q * jnp.exp(cumulative)
        scores = (
            jnp.einsum("ihd,jhd->hij", query_dec, block_k * jnp.exp(-cumulative), precision=precise)
            * triangle
        )
        result = jnp.einsum("hij,jhe->ihe", scores, block_v, precision=precise)
        result = result + jnp.einsum("ihd,hde->ihe", query_dec, state_now, precision=precise)
        state_next = state_now * jnp.exp(block_end)[:, :, None] + jnp.einsum(
            "jhd,jhe->hde", block_k * jnp.exp(block_end - cumulative), block_v, precision=precise
        )
        return (state_next, result)

    _, outputs = lax.scan(
        advance, carried, (shaped(queries), shaped(key_rows), shaped(value_rows), shaped(log_decay))
    )
    return outputs.reshape(length, head_count, value_width)


def head_channels(pieces, per_head, tp_index):
    for bit_number in range(per_head.bit_length() - 1):
        partner = from_partner(
            (for_sending(pieces[0]), for_sending(pieces[1]), for_sending(pieces[2])),
            "tp",
            bit_number,
        )
        upper = tp_index // (1 << bit_number) % 2 == 1
        pieces = tuple(
            (
                jnp.where(
                    upper,
                    jnp.concatenate([theirs, mine], axis=1),
                    jnp.concatenate([mine, theirs], axis=1),
                )
                for mine, theirs in zip(pieces, partner)
            )
        )
    return pieces


def context_totals(fwd_growth, fwd_state, bwd_growth, bwd_state, identity):

    def absorb(carried, piece):
        return (combine(carried, piece), None)

    total_fwd, _ = lax.scan(absorb, identity, (fwd_growth, fwd_state))
    total_bwd, _ = lax.scan(absorb, identity, (bwd_growth, bwd_state), reverse=True)
    return (total_fwd, total_bwd)


def stored(array):
    return lax.optimization_barrier(array.astype(jnp.bfloat16))


def local(
    latent,
    context,
    conditioning,
    context_prompt_vector,
    shift_matrix,
    scale_matrix,
    residual_gate_matrix,
    query_matrix,
    key_matrix,
    value_matrix,
    gate_matrix,
    decay_down_factor,
    decay_up_factor,
    decay_key_bias,
    spike_log_decay,
    output_gain,
    output_matrix,
):
    tp_count = lax.axis_size("tp")
    tp_index = lax.axis_index("tp")
    per_head = max(tp_count // HEADS, 1)
    heads_per_shard = max(HEADS // tp_count, 1)
    leading_head = tp_index // per_head * heads_per_shard
    tok_rows = latent.shape[0]
    conds = jax.nn.silu(
        jnp.stack([conditioning, context_prompt_vector]).astype(jnp.float32)
    ).astype(jnp.bfloat16)
    shifts, scales, gates = lax.psum(
        (
            linear(conds, shift_matrix),
            linear(conds, scale_matrix),
            linear(conds, residual_gate_matrix),
        ),
        "sp",
    )
    down_both = jnp.concatenate([decay_down_factor[0].T, decay_down_factor[1].T], axis=0)
    lat_weights = (query_matrix, key_matrix, value_matrix, gate_matrix, down_both)
    ctx_weights = (key_matrix, value_matrix, down_both)
    lat_f = latent.astype(jnp.float32)
    ctx_f = context.astype(jnp.float32)
    lat_sum, lat_squares, ctx_sum, ctx_squares = lax.psum(
        (
            jnp.sum(lat_f, axis=1, keepdims=True),
            jnp.sum(lat_f * lat_f, axis=1, keepdims=True),
            jnp.sum(ctx_f, axis=1, keepdims=True),
            jnp.sum(ctx_f * ctx_f, axis=1, keepdims=True),
        ),
        "tp",
    )
    latent_normalized = modulated(latent, lat_sum, lat_squares, shifts[0], scales[0])
    normed_ctx = modulated(context, ctx_sum, ctx_squares, shifts[1], scales[1])
    lat_piece = lax.all_gather(latent_normalized, "tp", axis=1, tiled=True)
    ctx_piece = lax.all_gather(normed_ctx, "tp", axis=1, tiled=True)
    lat_new = tuple((linear(lat_piece, weight) for weight in lat_weights))
    ctx_new = tuple((linear(ctx_piece, weight) for weight in ctx_weights))
    query_part, key_part, value_part, gate_part, low_rank_part = lat_new
    ctx_key_part, ctx_value_part, ctx_low = ctx_new
    query_full, key_full, ctx_key_full = head_channels(
        (stored(query_part), stored(key_part), stored(ctx_key_part)), per_head, tp_index
    )

    def split_heads(rows, width):
        return rows.astype(jnp.float32).reshape(rows.shape[0], heads_per_shard, width)

    value_cols = value_part.shape[1] // heads_per_shard
    queries = split_heads(query_full, DK) * DK ** (-0.5)
    key_rows = split_heads(key_full, DK)
    ctx_keys = split_heads(ctx_key_full, DK)
    values_lat = split_heads(stored(value_part), value_cols)
    values_ctx = split_heads(stored(ctx_value_part), value_cols)
    gate_rows = stored(gate_part).astype(jnp.float32)

    def per_head_decay(low_rows, direction):
        up_part = lax.dynamic_slice_in_dim(
            decay_up_factor[direction], leading_head * DK, heads_per_shard * DK, 1
        ).astype(jnp.float32)
        bias_part = lax.dynamic_slice_in_dim(
            decay_key_bias[direction], leading_head * DK, heads_per_shard * DK, 0
        )
        pre_act = jnp.dot(low_rows, up_part, precision=precise) + bias_part
        return (jax.nn.log_sigmoid(pre_act) / gate_norm).reshape(
            low_rows.shape[0], heads_per_shard, DK
        )

    decay_spikes = lax.dynamic_slice_in_dim(spike_log_decay, leading_head, heads_per_shard, 2)
    latent_forward = per_head_decay(low_rank_part[:, :DECAY_RANK], 0) + decay_spikes[0][:, :, None]
    latent_backward = per_head_decay(low_rank_part[:, DECAY_RANK:], 1) + decay_spikes[1][:, :, None]
    ctx_fwd = per_head_decay(ctx_low[:, :DECAY_RANK], 0)
    ctx_bwd = per_head_decay(ctx_low[:, DECAY_RANK:], 1)
    cf_growth, cf_state = end_state(ctx_keys, values_ctx, ctx_fwd)
    cb_growth, cb_state = end_state(
        reverse_rows(ctx_keys), reverse_rows(values_ctx), reverse_rows(ctx_bwd)
    )
    lf_growth, lf_state = end_state(key_rows, values_lat, latent_forward)
    lb_growth, lb_state = end_state(
        reverse_rows(key_rows), reverse_rows(values_lat), reverse_rows(latent_backward)
    )
    identity = (
        jnp.ones((heads_per_shard, DK), jnp.float32),
        jnp.zeros((heads_per_shard, DK, value_cols), jnp.float32),
    )
    ctx_gathered = (
        lax.all_gather(cf_growth[None].astype(jnp.bfloat16), "sp", axis=0, tiled=True).astype(
            jnp.float32
        ),
        lax.all_gather(cf_state[None].astype(jnp.bfloat16), "sp", axis=0, tiled=True).astype(
            jnp.float32
        ),
        lax.all_gather(cb_growth[None].astype(jnp.bfloat16), "sp", axis=0, tiled=True).astype(
            jnp.float32
        ),
        lax.all_gather(cb_state[None].astype(jnp.bfloat16), "sp", axis=0, tiled=True).astype(
            jnp.float32
        ),
    )
    total_fwd, total_bwd = context_totals(
        ctx_gathered[0], ctx_gathered[1], ctx_gathered[2], ctx_gathered[3], identity
    )
    prefix = carried_in((lf_growth, lf_state), "sp", combine, identity, False)
    suffix = carried_in((lb_growth, lb_state), "sp", combine, identity, True)
    start_fwd = combine(total_fwd, prefix)[1]
    start_bwd = combine(total_bwd, suffix)[1]
    zero_state = jnp.zeros((heads_per_shard, DK, value_cols), jnp.float32)

    def direction_out(query_rows, key_list, value_list, log_decay, start_state):
        local_part = blockwise(query_rows, key_list, value_list, log_decay, zero_state, BLK)
        reach = query_rows * jnp.exp(jnp.cumsum(log_decay, axis=0))
        return local_part + jnp.einsum("nhd,hde->nhe", reach, start_state, precision=precise)

    out_fwd = direction_out(queries, key_rows, values_lat, latent_forward, start_fwd)
    out_bwd = reverse_rows(
        direction_out(
            reverse_rows(queries),
            reverse_rows(key_rows),
            reverse_rows(values_lat),
            reverse_rows(latent_backward),
            start_bwd,
        )
    )
    grouped = (out_fwd + out_bwd).reshape(tok_rows, -1, VGROUP)
    grouped = grouped * lax.rsqrt(jnp.mean(grouped * grouped, axis=-1, keepdims=True) + epsilon)
    heads_out = (grouped.reshape(tok_rows, -1) * output_gain * jax.nn.silu(gate_rows)).astype(
        jnp.bfloat16
    )
    branch = linear(lax.all_gather(heads_out, "tp", axis=1, tiled=True), output_matrix)
    return (latent.astype(jnp.float32) + gates[0] * branch).astype(jnp.bfloat16)


def solution(mesh):
    placed = (
        P("sp", "tp"),
        P("sp", "tp"),
        P("sp"),
        P("sp"),
        P("tp", "sp"),
        P("tp", "sp"),
        P("tp", "sp"),
        P("tp", None),
        P("tp", None),
        P("tp", None),
        P("tp", None),
        P(),
        P(),
        P(),
        P(None, "sp", None),
        P("tp"),
        P("tp", None),
    )
    return jax.shard_map(
        local, mesh=mesh, in_specs=placed, out_specs=P("sp", "tp"), check_vma=False
    )
```

profile of v0, /device:TPU:0, one launch (start us, length us, event | category | flops | bytes accessed | tf_op | source)
XLA Modules:
  0.0 266.8 jit_solution(12194387579442730119)
XLA Ops:
  14.8 13.2 %all-reduce.1 = (f32[2,512]{1,0:T(2,128)S(1)}, f32[2,512]{1,0:T(2,128)S(1)}, f32[2,512]{1,0:T(2,128)}) all-reduce(f32[2,512]{1,0:T(2,128)S(1)} %fusion.121, f32[2,512]{1,0:T(2,128)S(1)} %fusion.123, f32[2,512]{1,0:T(2,128)S(1)} %fusion.125), channel_id=1, replica_groups=mesh['sp'=4,'tp'=8] {'sp'}, use_global_device_ids=true, to_apply=%region_6.7 | all-reduce | flops 3072 | bytes 24576 | tf_op jit(solution)/shard_map/psum | solution.py:178
  28.0 21.7 %all-reduce = (f32[128,1]{0,1:T(1,128)S(1)}, f32[128,1]{0,1:T(1,128)S(1)}, f32[16,1]{0,1:T(1,128)S(1)}, f32[16,1]{0,1:T(1,128)S(1)}) all-reduce(f32[128,1]{0,1:T(1,128)S(1)} %bitcast.291, f32[128,1]{0,1:T(1,128)S(1)} %bitcast.290, f32[16,1]{0,1:T(1,128)S(1)} %bitcast.293, f32[16,1]{0,1:T(1,128)S(1)} %bitcast.292), channel_id=1, replica_groups=mesh['sp'=4,'tp'=8] {'tp'}, use_global_device_ids=true, to_apply=%region_4.5 | all-reduce | flops 288 | bytes 2304 | tf_op jit(solution)/shard_map/psum | solution.py:191
  49.7 1.7 fusion.62
  53.5 31.0 %all_gather.45 = bf16[16,4096]{1,0:T(8,128)(2,1)S(1)} all-gather(bf16[16,512]{1,0:T(8,128)(2,1)S(1)} %fusion.89), channel_id=1, replica_groups=mesh['sp'=4,'tp'=8] {'tp'}, dimensions={1}, use_global_device_ids=true | all-gather | bytes 147456 | tf_op jit(solution)/shard_map/all_gather | solution.py:203
  84.9 3.4 %convolution_convert_fusion.8 = bf16[16,512]{1,0:T(8,128)(2,1)S(1)} fusion(bf16[16,4096]{1,0:T(8,128)(2,1)S(1)} %all_gather.45, bf16[512,4096]{1,0:T(8,128)(2,1)} %param.38), kind=kOutput, calls=%fused_computation.96 | convolution fusion | flops 67117056 | bytes 4341760 | tf_op jit(solution)/shard_map/dot_general | solution.py:54
  89.8 5.1 %all_gather.46 = bf16[4,2,128]{2,1,0:T(2,128)(2,1)S(1)} all-gather(bf16[1,2,128]{2,1,0:T(2,128)(2,1)S(1)} %get-tuple-element.728), channel_id=1, replica_groups=mesh['sp'=4,'tp'=8] {'sp'}, dimensions={0}, use_global_device_ids=true | all-gather | bytes 2560 | tf_op jit(solution)/shard_map/all_gather | solution.py:253
  95.8 7.3 %all-gather.1 = bf16[8,128,256]{2,1,0:T(8,128)(2,1)S(1)} all-gather(bf16[2,128,256]{2,1,0:T(8,128)(2,1)S(1)} %convolution_convert_fusion.5), channel_id=3, replica_groups=mesh['sp'=4,'tp'=8] {'sp'}, dimensions={0}, use_global_device_ids=true | all-gather | bytes 655360 | tf_op jit(solution)/shard_map/all_gather | solution.py:256
  106.9 5.0 %all_gather.51 = bf16[4,2,128]{2,1,0:T(2,128)(2,1)S(1)} all-gather(bf16[1,2,128]{2,1,0:T(2,128)(2,1)S(1)} %get-tuple-element.734), channel_id=1, replica_groups=mesh['sp'=4,'tp'=8] {'sp'}, dimensions={0}, use_global_device_ids=true | all-gather | bytes 2560 | tf_op jit(solution)/shard_map/all_gather | solution.py:259
  113.8 7.5 %all-gather.3 = bf16[8,128,256]{2,1,0:T(8,128)(2,1)S(1)} all-gather(bf16[2,128,256]{2,1,0:T(8,128)(2,1)S(1)} %convolution_convert_fusion.4), channel_id=5, replica_groups=mesh['sp'=4,'tp'=8] {'sp'}, dimensions={0}, use_global_device_ids=true | all-gather | bytes 655360 | tf_op jit(solution)/shard_map/all_gather | solution.py:262
  122.4 4.4 %while.91 = (s32[]{:T(128)}, f32[2,128,256]{2,1,0:T(8,128)S(1)}, f32[4,2,128]{2,1,0:T(2,128)S(1)}, f32[4,2,128,256]{3,2,1,0:T(8,128)}, s32[]{:T(128)}, /*index=5*/s32[]{:T(128)}, s32[]{:T(128)}) while((s32[]{:T(128)}, f32[2,128,256]{2,1,0:T(8,128)S(1)}, f32[4,2,128]{2,1,0:T(2,128)S(1)}, f32[4,2,128,256]{3,2,1,0:T(8,128)}, ...), condition=%wide.region_28.29_spmd.clone, body=%wide.region_27.28_spmd.clone.sunk | while | flops 196612 | bytes 789619 | solution.py:142
  127.5 1.8 fusion.70
  129.3 1.7 fusion.74
  133.5 2.1 convolution_convert_fusion.7
  137.0 3.7 %convolution_convert_fusion.2 = bf16[128,512]{1,0:T(8,128)(2,1)S(1)} fusion(bf16[128,4096]{1,0:T(8,128)(2,1)S(1)} %copy-done.1, bf16[512,4096]{1,0:T(8,128)(2,1)} %param.38), kind=kOutput, calls=%fused_computation.85 | convolution fusion | flops 536936448 | bytes 5373952 | tf_op jit(solution)/shard_map/dot_general | solution.py:54
  142.3 3.1 %convolution_convert_fusion.6 = bf16[128,256]{1,0:T(8,128)(2,1)} fusion(bf16[128,4096]{1,0:T(8,128)(2,1)S(1)} %copy-done.1, bf16[256,4096]{1,0:T(8,128)(2,1)} %param.36), kind=kOutput, calls=%fused_computation.94 | convolution fusion | flops 268468224 | bytes 3211264 | tf_op jit(solution)/shard_map/dot_general | solution.py:54
  148.4 4.4 %convolution_convert_fusion = bf16[128,512]{1,0:T(8,128)(2,1)} fusion(bf16[128,4096]{1,0:T(8,128)(2,1)S(1)} %copy-done.1, bf16[512,4096]{1,0:T(8,128)(2,1)} %param.39), kind=kOutput, calls=%fused_computation.83 | convolution fusion | flops 536936448 | bytes 5373952 | tf_op jit(solution)/shard_map/dot_general | solution.py:54
  158.9 2.3 exponential_multiply_fusion.2
  161.9 5.9 %while.89 = (s32[]{:T(128)}, f32[2,128,256]{2,1,0:T(8,128)S(1)}, f32[2,64,2,256]{3,1,0,2:T(8,128)}, f32[2,64,2,128]{3,2,1,0:T(2,128)S(1)}, f32[2,64,2,128]{3,2,1...) while((s32[]{:T(128)}, f32[2,128,256]{2,1,0:T(8,128)S(1)}, ...), condition=%wide.region_22.23_spmd.clone, body=%wide.region_20.22_spmd.clone.sunk | while | flops 139837440 | bytes 2366588 | solution.py:109
  167.8 1.9 copy.96
  169.7 5.1 %all_gather.48 = bf16[4,2,128]{2,1,0:T(2,128)(2,1)S(1)} all-gather(bf16[1,2,128]{2,1,0:T(2,128)(2,1)} %get-tuple-element.724), channel_id=1, replica_groups=mesh['sp'=4,'tp'=8] {'sp'}, dimensions={0}, use_global_device_ids=true | all-gather | bytes 2560 | tf_op jit(solution)/shard_map/all_gather | solution.py:32
  176.1 7.9 %all-gather.2 = bf16[8,128,256]{2,1,0:T(8,128)(2,1)} all-gather(bf16[2,128,256]{2,1,0:T(8,128)(2,1)S(1)} %convolution_convert_fusion.1), channel_id=4, replica_groups=mesh['sp'=4,'tp'=8] {'sp'}, dimensions={0}, use_global_device_ids=true | all-gather | bytes 655360 | tf_op jit(solution)/shard_map/all_gather | solution.py:32
  184.0 4.4 %while.90 = (s32[]{:T(128)}, f32[2,128]{1,0:T(2,128)S(1)}, f32[2,128,256]{2,1,0:T(8,128)S(1)}, s32[]{:T(128)}, bf16[4,2,128]{2,1,0:T(2,128)(2,1)S(1)}, /*index=5...) while((s32[]{:T(128)}, f32[2,128]{1,0:T(2,128)S(1)}, ...), condition=%wide.region_25.26_spmd.clone, body=%wide.region_24.25_spmd.clone.sunk | while | flops 328968 | bytes 660669 | solution.py:50
  188.4 2.4 fusion.46
  190.8 3.1 %rev.38 = f32[128,2,256]{0,2,1:T(8,128)} reverse(f32[128,2,256]{0,2,1:T(8,128)} %fusion.46), dimensions={0} | reverse | bytes 524288 | tf_op jit(solution)/shard_map/jit(_flip)/rev | solution.py:69
  195.8 4.3 %while.86 = (s32[]{:T(128)}, f32[2,128,256]{2,1,0:T(8,128)S(1)}, f32[2,64,2,256]{3,1,0,2:T(8,128)}, f32[2,64,2,128]{3,2,1,0:T(2,128)S(1)}, f32[2,64,2,128]{3,2,1...) while((s32[]{:T(128)}, f32[2,128,256]{2,1,0:T(8,128)S(1)}, ...), condition=%wide.region_9.10_spmd.clone, body=%wide.region_7.9_spmd.clone.sunk | while | flops 139837440 | bytes 2594944 | solution.py:109
  200.1 1.8 copy.86
  201.9 5.0 %all_gather.42 = bf16[4,2,128]{2,1,0:T(2,128)(2,1)S(1)} all-gather(bf16[1,2,128]{2,1,0:T(2,128)(2,1)S(1)} %get-tuple-element.720), channel_id=1, replica_groups=mesh['sp'=4,'tp'=8] {'sp'}, dimensions={0}, use_global_device_ids=true | all-gather | bytes 2560 | tf_op jit(solution)/shard_map/all_gather | solution.py:32
  207.3 7.6 %all-gather = bf16[8,128,256]{2,1,0:T(8,128)(2,1)S(1)} all-gather(bf16[2,128,256]{2,1,0:T(8,128)(2,1)S(1)} %convolution_convert_fusion.3), channel_id=2, replica_groups=mesh['sp'=4,'tp'=8] {'sp'}, dimensions={0}, use_global_device_ids=true | all-gather | bytes 655360 | tf_op jit(solution)/shard_map/all_gather | solution.py:32
  215.7 1.7 fusion.130
  217.8 1.7 fusion.68
  219.5 35.8 %all-gather.9.cloned.1.call-done = bf16[128,4096]{1,0:T(8,128)(2,1)} async-done(((bf16[128,512]{1,0:T(8,128)(2,1)}), bf16[128,4096]{1,0:T(8,128)(2,1)}) %all-gather.9.cloned.1.call-update) | async-done | bytes 1048592 | tf_op jit(solution)/shard_map/all_gather | solution.py:295
  255.3 4.7 %fusion.50 = bf16[128,512]{1,0:T(8,128)(2,1)} fusion(bf16[128,4096]{1,0:T(8,128)(2,1)} %all-gather.9.cloned.1.call-done, bf16[512,4096]{1,0:T(8,128)(2,1)} %param.45, bf16[128,512]{1,0:T(8,128)(2,1)S(1)} %copy-done.11, f32[512]{0:T(512)S(1)} %bitcast.285), kind=kOutput, calls=%fused_computation.87 | convolution fusion | flops 537133056 | bytes 5507072 | tf_op jit(solution)/shard_map/dot_general | solution.py:54
  (210 shorter events, 60.2 us)
Async XLA Ops:
  6.5 82.4 %copy-start = (bf16[256,4096]{1,0:T(8,128)(2,1)S(1)}, bf16[256,4096]{1,0:T(8,128)(2,1)}, u32[]{:S(2)}) copy-start(bf16[256,4096]{1,0:T(8,128)(2,1)} %param.37) | copy-start | bytes 6291460
  6.5 46.8 %copy-start.17 = (bf16[16,512]{1,0:T(8,128)(2,1)S(1)}, bf16[16,512]{1,0:T(8,128)(2,1)}, u32[]{:S(2)}) copy-start(bf16[16,512]{1,0:T(8,128)(2,1)} %param.30) | copy-start | bytes 49156
  6.5 46.7 %copy-start.16 = (bf16[2,16,2048]{2,1,0:T(8,128)(2,1)S(1)}, bf16[2,16,2048]{2,1,0:T(8,128)(2,1)}, u32[]{:S(2)}) copy-start(bf16[2,16,2048]{2,1,0:T(8,128)(2,1)} %param.41) | copy-start | bytes 393220
  6.5 121.0 %all-gather.7.cloned.1.call-start = ((), (), s32[]{:S(2)}) async-start(), calls=%async_computation | async-start | bytes 1179648 | tf_op jit(solution)/shard_map/all_gather | solution.py:202
  51.4 203.9 %all-gather.9.cloned.1.call-start = ((), (), s32[]{:S(2)}) async-start(), calls=%async_computation.1 | async-start | bytes 1179648 | tf_op jit(solution)/shard_map/all_gather | solution.py:295
  53.3 49.8 %copy-start.15 = (bf16[16,4096]{1,0:T(8,128)(2,1)}, bf16[16,4096]{1,0:T(8,128)(2,1)S(1)}, u32[]{:S(2)}) copy-start(bf16[16,4096]{1,0:T(8,128)(2,1)S(1)} %get-tuple-element.713) | copy-start | bytes 393220
  53.3 49.8 %copy-start.18 = (bf16[1,16,2048]{2,1,0:T(8,128)(2,1)}, bf16[1,16,2048]{2,1,0:T(8,128)(2,1)S(1)}, u32[]{:S(2)}) copy-start(bf16[1,16,2048]{2,1,0:T(8,128)(2,1)S(1)} %get-tuple-element.721) | copy-start | bytes 196612
  53.3 49.8 %copy-start.19 = (bf16[1,16,2048]{2,1,0:T(8,128)(2,1)}, bf16[1,16,2048]{2,1,0:T(8,128)(2,1)S(1)}, u32[]{:S(2)}) copy-start(bf16[1,16,2048]{2,1,0:T(8,128)(2,1)S(1)} %get-tuple-element.722) | copy-start | bytes 196612
  84.4 5.4 %copy-start.22 = (f32[1,256]{1,0:T(1,128)}, f32[1,256]{1,0:T(1,128)S(1)}, u32[]{:S(2)}) copy-start(f32[1,256]{1,0:T(1,128)S(1)} %get-tuple-element.747) | copy-start | bytes 3076
  103.9 0.8 copy-start.3
  126.8 0.7 copy-start.5
  127.5 9.4 %copy-start.1 = (bf16[128,4096]{1,0:T(8,128)(2,1)S(1)}, bf16[128,4096]{1,0:T(8,128)(2,1)}, u32[]{:S(2)}) copy-start(bf16[128,4096]{1,0:T(8,128)(2,1)} %all-gather.7.cloned.1.call-done) | copy-start | bytes 3145732
  152.8 9.1 %copy-start.2 = (f32[2,128,256]{2,1,0:T(8,128)S(1)}, f32[2,128,256]{2,1,0:T(8,128)}, u32[]{:S(2)}) copy-start(f32[2,128,256]{2,1,0:T(8,128)} %custom-call.4) | copy-start | bytes 786436
  161.9 22.1 %copy-start.8 = (f32[2,128,256]{2,1,0:T(8,128)S(1)}, f32[2,128,256]{2,1,0:T(8,128)}, u32[]{:S(2)}) copy-start(f32[2,128,256]{2,1,0:T(8,128)} %custom-call.6) | copy-start | bytes 786436
  167.8 20.6 %copy-start.6 = (f32[2,128,256]{2,1,0:T(8,128)S(1)}, f32[2,128,256]{2,1,0:T(8,128)}, u32[]{:S(2)}) copy-start(f32[2,128,256]{2,1,0:T(8,128)} %copy-done.5) | copy-start | bytes 786436
  167.8 28.0 %copy-start.9 = (f32[2,64,2,256]{3,2,1,0:T(2,128)S(1)}, f32[2,64,2,256]{3,2,1,0:T(2,128)}, u32[]{:S(2)}) copy-start(f32[2,64,2,256]{3,2,1,0:T(2,128)} %reshape_reshape.7) | copy-start | bytes 786436
  176.1 17.8 %copy-start.14 = (f32[128,256]{1,0:T(8,128)S(1)}, f32[128,256]{1,0:T(8,128)}, u32[]{:S(2)}) copy-start(f32[128,256]{1,0:T(8,128)} %broadcast_multiply_fusion) | copy-start | bytes 393220
  176.1 19.7 %copy-start.10 = (f32[2,64,2,128]{3,2,1,0:T(2,128)S(1)}, f32[2,64,2,128]{3,2,1,0:T(2,128)}, u32[]{:S(2)}) copy-start(f32[2,64,2,128]{3,2,1,0:T(2,128)} %reshape_reshape.6) | copy-start | bytes 393220
  195.8 11.2 %copy-start.13 = (f32[128,2,128]{2,1,0:T(2,128)S(1)}, f32[128,2,128]{2,1,0:T(2,128)}, u32[]{:S(2)}) copy-start(f32[128,2,128]{2,1,0:T(2,128)} %get-tuple-element.717) | copy-start | bytes 393220
  195.8 19.2 %copy-start.7 = (f32[2,128,256]{2,1,0:T(8,128)S(1)}, f32[2,128,256]{2,1,0:T(8,128)}, u32[]{:S(2)}) copy-start(f32[2,128,256]{2,1,0:T(8,128)} %custom-call.2) | copy-start | bytes 786436
  200.1 15.6 %copy-start.4 = (f32[2,128,256]{2,1,0:T(8,128)S(1)}, f32[2,128,256]{2,1,0:T(8,128)}, u32[]{:S(2)}) copy-start(f32[2,128,256]{2,1,0:T(8,128)} %copy-done.3) | copy-start | bytes 786436
  200.1 17.7 %copy-start.20 = (f32[512]{0:T(512)S(1)}, f32[512]{0:T(512)}, u32[]{:S(2)}) copy-start(f32[512]{0:T(512)} %param.44) | copy-start | bytes 6148
  207.3 8.4 %copy-start.12 = (f32[128,2,256]{0,2,1:T(8,128)S(1)}, f32[128,2,256]{0,2,1:T(8,128)}, u32[]{:S(2)}) copy-start(f32[128,2,256]{0,2,1:T(8,128)} %rev.38) | copy-start | bytes 786436
  207.3 12.2 %copy-start.21 = (f32[2,512]{1,0:T(2,128)S(1)}, f32[2,512]{1,0:T(2,128)}, u32[]{:S(2)}) copy-start(f32[2,512]{1,0:T(2,128)} %get-tuple-element.705) | copy-start | bytes 12292
  207.3 47.9 %copy-start.11 = (bf16[128,512]{1,0:T(8,128)(2,1)S(1)}, bf16[128,512]{1,0:T(8,128)(2,1)}, u32[]{:S(2)}) copy-start(bf16[128,512]{1,0:T(8,128)(2,1)} %param.29) | copy-start | bytes 393220
Sparse Core Ops, SparseCore 0:
  51.5 35.1 all-gather.6
  219.6 35.6 all-gather.8
where the time goes:
time: 269 us; the launch traced here: 267 us
  blocking collectives  116 us (43%)
  matrix products  46.5 us (17%)
  waiting for transfers between devices  35.8 us (13%)
  other arithmetic  28.5 us (11%)
  local copies, waits for them, and re-layouts  25 us (9%)
  between operations  13.9 us (5%)
    all_gather x1, waiting for transfers between devices, local(): lax.all_gather(heads_out, 'tp', axis=1, tiled=True)  35.8 us
    all_gather x1, blocking collectives, local(): ctx_piece = lax.all_gather(normed_ctx, 'tp', axis=1, tiled=True)  31 us
    dot_general x12, matrix products, linear(): lax.dot_general(rows, weight, (((1,), (1,)), ((), ())), preferred_element...  28.7 us
    all_gather x4, blocking collectives, carried_in(): lax.all_gather(part.astype(kind), axis)  25.6 us
    psum x1, blocking collectives, local(): lax.psum((jnp.sum(lat_f, axis=1, keepdims=True), jnp.sum(lat_f * lat_f, a...  21.7 us
    psum x1, blocking collectives, local(): lax.psum((linear(conds, shift_matrix), linear(conds, scale_matrix), linea...  13.2 us
    all_gather x1, blocking collectives, local(): lax.all_gather(cb_state[None].astype(jnp.bfloat16), 'sp', axis=0, tiled=T...  7.46 us
    all_gather x1, blocking collectives, local(): lax.all_gather(cf_state[None].astype(jnp.bfloat16), 'sp', axis=0, tiled=T...  7.28 us
  transfers between devices with their start and end apart: 2, of which 1 were waited for; matrix products, arithmetic and copies ran while one was open for 7% of the time, Pallas kernels for 0%

commit v1 on v0

--- a/solution.py
+++ b/solution.py
@@ -199,8 +199,13 @@
     )
     latent_normalized = modulated(latent, lat_sum, lat_squares, shifts[0], scales[0])
     normed_ctx = modulated(context, ctx_sum, ctx_squares, shifts[1], scales[1])
-    lat_piece = lax.all_gather(latent_normalized, "tp", axis=1, tiled=True)
-    ctx_piece = lax.all_gather(normed_ctx, "tp", axis=1, tiled=True)
+    lat_piece, ctx_piece = jnp.split(
+        lax.all_gather(
+            jnp.concatenate([latent_normalized, normed_ctx], axis=0), "tp", axis=1, tiled=True
+        ),
+        [latent_normalized.shape[0]],
+        axis=0,
+    )
     lat_new = tuple((linear(lat_piece, weight) for weight in lat_weights))
     ctx_new = tuple((linear(ctx_piece, weight) for weight in ctx_weights))
     query_part, key_part, value_part, gate_part, low_rank_part = lat_new

time: 269 us -> 297 us (1.10)
  waiting for transfers between devices: 35.8 us -> 66.9 us
  blocking collectives: 116 us -> 85.5 us
  other arithmetic: 28.5 us -> 47.2 us
  local copies, waits for them, and re-layouts: 25 us -> 30.7 us
  matrix products: 46.5 us -> 50.5 us
    all_gather x1 -> x0, blocking collectives: 31 us -> none  [local(): ctx_piece = lax.all_gather(normed_ctx, 'tp', axis=1, tiled=True)]
    all_gather x1, waiting for transfers between devices: 0.01 us -> 29.3 us  [local(): lax.all_gather(jnp.concatenate([latent_normalized, normed_ctx], axis=0),...]
    select_n x16, other arithmetic: 4.76 us -> 15.7 us  [turn(): return jax.tree.map(lambda a, b: jnp.where(reached, a, b), new, before)]
    mul x8, local copies, waits for them, and re-layouts: 0.05 us -> 5.09 us  [combine(): return (earlier[0] * later[0], later[0][..., None] * earlier[1] + later[1])]
    add x8, other arithmetic: 4.77 us -> 8.58 us  [combine(): return (earlier[0] * later[0], later[0][..., None] * earlier[1] + later[1])]
    mul x4, other arithmetic: 2.14 us -> 5.19 us  [advance(): block_k * jnp.exp(-cumulative)]
  transfers between devices with their start and end apart: 2 -> 2, of which waited for: 1 -> 2; matrix products, arithmetic and copies ran while one was open for 7% -> 2% of each run, Pallas kernels for 0% -> 0%
where the time goes in v1:
time: 297 us; the launch traced here: 295 us
  blocking collectives  85.5 us (29%)
  waiting for transfers between devices  66.9 us (23%)
  matrix products  50.5 us (17%)
  other arithmetic  47.2 us (16%)
  local copies, waits for them, and re-layouts  30.7 us (10%)
  between operations  13.9 us (5%)
    all_gather x1, waiting for transfers between devices, local(): lax.all_gather(heads_out, 'tp', axis=1, tiled=True)  37.5 us
    all_gather x1, waiting for transfers between devices, local(): lax.all_gather(jnp.concatenate([latent_normalized, normed_ctx], axis=0),...  29.3 us
    dot_general x12, matrix products, linear(): lax.dot_general(rows, weight, (((1,), (1,)), ((), ())), preferred_element...  29.1 us
    all_gather x4, blocking collectives, carried_in(): lax.all_gather(part.astype(kind), axis)  25.9 us
    psum x1, blocking collectives, local(): lax.psum((jnp.sum(lat_f, axis=1, keepdims=True), jnp.sum(lat_f * lat_f, a...  21.7 us
    select_n x16, other arithmetic, turn(): return jax.tree.map(lambda a, b: jnp.where(reached, a, b), new, before)  15.7 us
    psum x1, blocking collectives, local(): lax.psum((linear(conds, shift_matrix), linear(conds, scale_matrix), linea...  13.2 us
    add x8, other arithmetic, combine(): return (earlier[0] * later[0], later[0][..., None] * earlier[1] + later[1])  8.58 us
  transfers between devices with their start and end apart: 2, of which 2 were waited for; matrix products, arithmetic and copies ran while one was open for 2% of the time, Pallas kernels for 0%

profile of v1, /device:TPU:0, one launch (start us, length us, event | category | flops | bytes accessed | tf_op | source)
XLA Modules:
  0.0 295.4 jit_solution(15310089131585230253)
XLA Ops:
  12.1 13.2 %all-reduce.1 = (f32[2,512]{1,0:T(2,128)S(1)}, f32[2,512]{1,0:T(2,128)S(1)}, f32[2,512]{1,0:T(2,128)}) all-reduce(f32[2,512]{1,0:T(2,128)S(1)} %fusion.129, f32[2,512]{1,0:T(2,128)S(1)} %fusion.131, f32[2,512]{1,0:T(2,128)S(1)} %fusion.133), channel_id=1, replica_groups=mesh['sp'=4,'tp'=8] {'sp'}, use_global_device_ids=true, to_apply=%region_6.7 | all-reduce | flops 3072 | bytes 24576 | tf_op jit(solution)/shard_map/psum | solution.py:178
  25.3 21.7 %all-reduce = (f32[16,1]{0,1:T(1,128)S(1)}, f32[16,1]{0,1:T(1,128)S(1)}, f32[128,1]{0,1:T(1,128)S(1)}, f32[128,1]{0,1:T(1,128)S(1)}) all-reduce(f32[16,1]{0,1:T(1,128)S(1)} %bitcast.283, f32[16,1]{0,1:T(1,128)S(1)} %bitcast.282, f32[128,1]{0,1:T(1,128)S(1)} %bitcast.281, ...), channel_id=1, replica_groups=mesh['sp'=4,'tp'=8] {'tp'}, use_global_device_ids=true, to_apply=%region_10.11 | all-reduce | flops 288 | bytes 2304 | tf_op jit(solution)/shard_map/psum | solution.py:191
  54.9 29.3 %all-gather.7.cloned.1.call-done = bf16[144,4096]{1,0:T(8,128)(2,1)} async-done(((bf16[144,512]{1,0:T(8,128)(2,1)}), bf16[144,4096]{1,0:T(8,128)(2,1)}) %all-gather.7.cloned.1.call-update) | async-done | bytes 1179664 | tf_op jit(solution)/shard_map/all_gather | solution.py:203
  93.1 4.0 %convolution_convert_fusion.2 = bf16[128,512]{1,0:T(8,128)(2,1)S(1)} fusion(bf16[512,4096]{1,0:T(8,128)(2,1)} %param.38, bf16[144,4096]{1,0:T(8,128)(2,1)} %all-gather.7.cloned.1.call-done), kind=kOutput, calls=%fused_computation.85 | convolution fusion | flops 536936448 | bytes 5373952 | tf_op jit(solution)/shard_map/dot_general | solution.py:54
  98.8 2.8 convolution_convert_fusion.6
  102.9 2.1 convolution_convert_fusion.7
  108.0 3.5 %convolution_convert_fusion.8 = bf16[16,512]{1,0:T(8,128)(2,1)S(1)} fusion(bf16[512,4096]{1,0:T(8,128)(2,1)} %param.38, bf16[144,4096]{1,0:T(8,128)(2,1)} %all-gather.7.cloned.1.call-done), kind=kOutput, calls=%fused_computation.96 | convolution fusion | flops 67117056 | bytes 4341760 | tf_op jit(solution)/shard_map/dot_general | solution.py:54
  112.6 7.3 %all-gather.3 = bf16[8,128,256]{2,1,0:T(8,128)(2,1)S(1)} all-gather(bf16[2,128,256]{2,1,0:T(8,128)(2,1)S(1)} %convolution_convert_fusion.4), channel_id=5, replica_groups=mesh['sp'=4,'tp'=8] {'sp'}, dimensions={0}, use_global_device_ids=true | all-gather | bytes 655360 | tf_op jit(solution)/shard_map/all_gather | solution.py:267
  120.9 5.0 %all_gather.47 = bf16[4,2,128]{2,1,0:T(2,128)(2,1)S(1)} all-gather(bf16[1,2,128]{2,1,0:T(2,128)(2,1)S(1)} %get-tuple-element.734), channel_id=1, replica_groups=mesh['sp'=4,'tp'=8] {'sp'}, dimensions={0}, use_global_device_ids=true | all-gather | bytes 2560 | tf_op jit(solution)/shard_map/all_gather | solution.py:264
  126.6 9.4 %while.91 = (s32[]{:T(128)}, f32[2,128,256]{2,1,0:T(8,128)S(1)}, f32[4,2,128]{2,1,0:T(2,128)}, f32[4,2,128,256]{3,2,1,0:T(8,128)}, s32[]{:T(128)}, /*index=5*/s32[]{:T(128)}, s32[]{:T(128)}) while((s32[]{:T(128)}, f32[2,128,256]{2,1,0:T(8,128)S(1)}, f32[4,2,128]{2,1,0:T(2,128)}, f32[4,2,128,256]{3,2,1,0:T(8,128)}, s32[]{:T(128)}, ...), condition=%wide.region_28.29_spmd.clone, body=%wide.region_27.28_spmd.clone.sunk | while | flops 196612 | bytes 789611 | solution.py:142
  140.0 1.8 broadcast_add_fusion
  148.1 2.3 exponential_multiply_fusion.2
  150.8 7.7 %all-gather.2 = bf16[8,128,256]{2,1,0:T(8,128)(2,1)} all-gather(bf16[2,128,256]{2,1,0:T(8,128)(2,1)S(1)} %convolution_convert_fusion.1), channel_id=4, replica_groups=mesh['sp'=4,'tp'=8] {'sp'}, dimensions={0}, use_global_device_ids=true | all-gather | bytes 655360 | tf_op jit(solution)/shard_map/all_gather | solution.py:32
  158.6 5.2 %all_gather.44 = bf16[4,2,128]{2,1,0:T(2,128)(2,1)S(1)} all-gather(bf16[1,2,128]{2,1,0:T(2,128)(2,1)S(1)} %copy-done.23), channel_id=1, replica_groups=mesh['sp'=4,'tp'=8] {'sp'}, dimensions={0}, use_global_device_ids=true | all-gather | bytes 2560 | tf_op jit(solution)/shard_map/all_gather | solution.py:32
  163.8 11.5 %while.90 = (s32[]{:T(128)}, f32[2,128]{1,0:T(2,128)}, f32[2,128,256]{2,1,0:T(8,128)}, s32[]{:T(128)}, bf16[4,2,128]{2,1,0:T(2,128)(2,1)S(1)}, /*index=5*/bf16[4...) while((s32[]{:T(128)}, f32[2,128]{1,0:T(2,128)}, ...), condition=%wide.region_25.26_spmd.clone, body=%wide.region_24.25_spmd.clone.sunk | while | flops 328968 | bytes 660661 | solution.py:50
  163.8 1.7 fusion.211
  166.1 1.8 fusion.211
  169.2 1.8 fusion.211
  172.2 1.8 fusion.211
  176.0 13.4 %while.89 = (s32[]{:T(128)}, f32[2,128,256]{2,1,0:T(8,128)S(1)}, f32[2,64,2,256]{3,1,0,2:T(8,128)}, f32[2,64,2,128]{3,2,1,0:T(2,128)}, f32[2,64,2,128]{3,2,1,0:T...) while((s32[]{:T(128)}, f32[2,128,256]{2,1,0:T(8,128)S(1)}, ...), condition=%wide.region_22.23_spmd.clone, body=%wide.region_20.22_spmd.clone.sunk | while | flops 139837440 | bytes 2367088 | solution.py:109
  179.7 1.8 fusion.210
  186.4 1.8 fusion.210
  194.1 7.3 %all-gather.1 = bf16[8,128,256]{2,1,0:T(8,128)(2,1)S(1)} all-gather(bf16[2,128,256]{2,1,0:T(8,128)(2,1)S(1)} %convolution_convert_fusion.5), channel_id=3, replica_groups=mesh['sp'=4,'tp'=8] {'sp'}, dimensions={0}, use_global_device_ids=true | all-gather | bytes 655360 | tf_op jit(solution)/shard_map/all_gather | solution.py:261
  202.4 5.2 %all_gather.42 = bf16[4,2,128]{2,1,0:T(2,128)(2,1)S(1)} all-gather(bf16[1,2,128]{2,1,0:T(2,128)(2,1)S(1)} %copy-done.21), channel_id=1, replica_groups=mesh['sp'=4,'tp'=8] {'sp'}, dimensions={0}, use_global_device_ids=true | all-gather | bytes 2560 | tf_op jit(solution)/shard_map/all_gather | solution.py:258
  207.6 4.5 %while.88 = (s32[]{:T(128)}, f32[2,128,256]{2,1,0:T(8,128)S(1)}, f32[4,2,128]{2,1,0:T(2,128)S(1)}, f32[4,2,128,256]{3,2,1,0:T(8,128)}, s32[]{:T(128)}, /*index=5*/s32[]{:T(128)}) while((s32[]{:T(128)}, f32[2,128,256]{2,1,0:T(8,128)S(1)}, f32[4,2,128]{2,1,0:T(2,128)S(1)}, f32[4,2,128,256]{3,2,1,0:T(8,128)}, s32[]{:T(128)}, ...), condition=%wide.region_19.20_spmd.clone, body=%wide.region_18.19_spmd.clone.sunk | while | flops 196611 | bytes 789591 | solution.py:141
  212.5 7.9 %all-gather = bf16[8,128,256]{2,1,0:T(8,128)(2,1)} all-gather(bf16[2,128,256]{2,1,0:T(8,128)(2,1)S(1)} %convolution_convert_fusion.3), channel_id=2, replica_groups=mesh['sp'=4,'tp'=8] {'sp'}, dimensions={0}, use_global_device_ids=true | all-gather | bytes 655360 | tf_op jit(solution)/shard_map/all_gather | solution.py:32
  220.3 5.0 %all_gather.39 = bf16[4,2,128]{2,1,0:T(2,128)(2,1)S(1)} all-gather(bf16[1,2,128]{2,1,0:T(2,128)(2,1)S(1)} %copy-done.22), channel_id=1, replica_groups=mesh['sp'=4,'tp'=8] {'sp'}, dimensions={0}, use_global_device_ids=true | all-gather | bytes 2560 | tf_op jit(solution)/shard_map/all_gather | solution.py:32
  225.4 4.4 %while.87 = (s32[]{:T(128)}, f32[2,128]{1,0:T(2,128)S(1)}, f32[2,128,256]{2,1,0:T(8,128)S(1)}, s32[]{:T(128)}, bf16[4,2,128]{2,1,0:T(2,128)(2,1)S(1)}, /*index=5...) while((s32[]{:T(128)}, f32[2,128]{1,0:T(2,128)S(1)}, f32[2,128,256]{2,1,0:T(8,128)S(1)}, ...), condition=%wide.region_16.17_spmd.clone, body=%wide.region_15.16_spmd.clone.sunk | while | flops 328964 | bytes 660599 | solution.py:50
  232.3 6.0 %while.86 = (s32[]{:T(128)}, f32[2,128,256]{2,1,0:T(8,128)S(1)}, f32[2,64,2,256]{3,1,0,2:T(8,128)}, f32[2,64,2,128]{3,2,1,0:T(2,128)S(1)}, f32[2,64,2,128]{3,2,1...) while((s32[]{:T(128)}, f32[2,128,256]{2,1,0:T(8,128)S(1)}, ...), condition=%wide.region_13.14_spmd.clone, body=%wide.region_11.13_spmd.clone.sunk | while | flops 139837440 | bytes 2595444 | solution.py:109
  241.5 4.1 %convolution_convert_fusion = bf16[128,512]{1,0:T(8,128)(2,1)S(1)} fusion(bf16[512,4096]{1,0:T(8,128)(2,1)} %param.39, bf16[144,4096]{1,0:T(8,128)(2,1)} %all-gather.7.cloned.1.call-done), kind=kOutput, calls=%fused_computation.83 | convolution fusion | flops 536936448 | bytes 5373952 | tf_op jit(solution)/shard_map/dot_general | solution.py:54
  246.3 37.5 %all-gather.9.cloned.1.call-done = bf16[128,4096]{1,0:T(8,128)(2,1)} async-done(((bf16[128,512]{1,0:T(8,128)(2,1)}), bf16[128,4096]{1,0:T(8,128)(2,1)}) %all-gather.9.cloned.1.call-update) | async-done | bytes 1048592 | tf_op jit(solution)/shard_map/all_gather | solution.py:300
  283.9 4.7 %fusion.50 = bf16[128,512]{1,0:T(8,128)(2,1)} fusion(bf16[128,4096]{1,0:T(8,128)(2,1)} %all-gather.9.cloned.1.call-done, bf16[512,4096]{1,0:T(8,128)(2,1)} %param.45, bf16[128,512]{1,0:T(8,128)(2,1)S(1)} %copy-done.6, f32[512]{0:T(512)S(1)} %bitcast.275), kind=kOutput, calls=%fused_computation.87 | convolution fusion | flops 537133056 | bytes 5507072 | tf_op jit(solution)/shard_map/dot_general | solution.py:54
  (214 shorter events, 92.7 us)
Async XLA Ops:
  6.5 96.4 %copy-start = (bf16[256,4096]{1,0:T(8,128)(2,1)S(1)}, bf16[256,4096]{1,0:T(8,128)(2,1)}, u32[]{:S(2)}) copy-start(bf16[256,4096]{1,0:T(8,128)(2,1)} %param.37) | copy-start | bytes 6291460
  6.5 5.3 %copy-start.5 = (bf16[128,512]{1,0:T(8,128)(2,1)S(1)}, bf16[128,512]{1,0:T(8,128)(2,1)}, u32[]{:S(2)}) copy-start(bf16[128,512]{1,0:T(8,128)(2,1)} %param.29) | copy-start | bytes 393220
  6.5 5.4 %copy-start.16 = (bf16[16,512]{1,0:T(8,128)(2,1)S(1)}, bf16[16,512]{1,0:T(8,128)(2,1)}, u32[]{:S(2)}) copy-start(bf16[16,512]{1,0:T(8,128)(2,1)} %param.30) | copy-start | bytes 49156
  6.5 77.7 %all-gather.7.cloned.1.call-start = ((), (), s32[]{:S(2)}) async-start(), calls=%async_computation | async-start | bytes 1327104 | tf_op jit(solution)/shard_map/all_gather | solution.py:203
  6.5 4.9 %copy-start.7 = (bf16[512,1024]{1,0:T(8,128)(2,1)S(1)}, bf16[512,1024]{1,0:T(8,128)(2,1)}, u32[]{:S(2)}) copy-start(bf16[512,1024]{1,0:T(8,128)(2,1)} %param.35) | copy-start | bytes 3145732
  8.1 45.4 %copy-start.19 = (f32[2,2048]{1,0:T(2,128)S(1)}, f32[2,2048]{1,0:T(2,128)}, u32[]{:S(2)}) copy-start(f32[2,2048]{1,0:T(2,128)} %param.42) | copy-start | bytes 49156
  8.2 45.5 %copy-start.15 = (bf16[2,16,2048]{2,1,0:T(8,128)(2,1)S(1)}, bf16[2,16,2048]{2,1,0:T(8,128)(2,1)}, u32[]{:S(2)}) copy-start(bf16[2,16,2048]{2,1,0:T(8,128)(2,1)} %param.41) | copy-start | bytes 393220
  9.8 44.5 %copy-start.14 = (bf16[2,4096,16]{1,2,0:T(8,128)(2,1)S(1)}, bf16[2,4096,16]{1,2,0:T(8,128)(2,1)}, u32[]{:S(2)}) copy-start(bf16[2,4096,16]{1,2,0:T(8,128)(2,1)} %param.40) | copy-start | bytes 786436
  47.9 236.0 %all-gather.9.cloned.1.call-start = ((), (), s32[]{:S(2)}) async-start(), calls=%async_computation.1 | async-start | bytes 1179648 | tf_op jit(solution)/shard_map/all_gather | solution.py:300
  97.1 5.1 %copy-start.3 = (bf16[128,512]{1,0:T(8,128)(2,1)}, bf16[128,512]{1,0:T(8,128)(2,1)S(1)}, u32[]{:S(2)}) copy-start(bf16[128,512]{1,0:T(8,128)(2,1)S(1)} %convolution_convert_fusion.2) | copy-start | bytes 393220
  126.6 18.4 %copy-start.8 = (f32[128,512]{1,0:T(8,128)S(1)}, f32[128,512]{1,0:T(8,128)}, u32[]{:S(2)}) copy-start(f32[128,512]{1,0:T(8,128)} %convert_element_type.181) | copy-start | bytes 786436
  137.1 0.6 copy-start.9
  144.4 1.3 copy-start.10
  148.1 10.4 %copy-start.23 = (bf16[1,2,128]{2,1,0:T(2,128)(2,1)S(1)}, bf16[1,2,128]{2,1,0:T(2,128)(2,1)}, u32[]{:S(2)}) copy-start(bf16[1,2,128]{2,1,0:T(2,128)(2,1)} %get-tuple-element.724) | copy-start | bytes 1540
  189.5 4.3 %copy-start.17 = (f32[16,2,128]{2,1,0:T(2,128)S(1)}, f32[16,2,128]{2,1,0:T(2,128)}, u32[]{:S(2)}) copy-start(f32[16,2,128]{2,1,0:T(2,128)} %get-tuple-element.725) | copy-start | bytes 49156
  190.6 11.9 %copy-start.21 = (bf16[1,2,128]{2,1,0:T(2,128)(2,1)S(1)}, bf16[1,2,128]{2,1,0:T(2,128)(2,1)}, u32[]{:S(2)}) copy-start(bf16[1,2,128]{2,1,0:T(2,128)(2,1)} %get-tuple-element.728) | copy-start | bytes 1540
  202.4 9.7 %copy-start.4 = (bf16[128,512]{1,0:T(8,128)(2,1)S(1)}, bf16[128,512]{1,0:T(8,128)(2,1)}, u32[]{:S(2)}) copy-start(bf16[128,512]{1,0:T(8,128)(2,1)} %copy-done.3) | copy-start | bytes 393220
  202.4 9.7 %copy-start.11 = (f32[128,2,128]{2,1,0:T(2,128)S(1)}, f32[128,2,128]{2,1,0:T(2,128)}, u32[]{:S(2)}) copy-start(f32[128,2,128]{2,1,0:T(2,128)} %get-tuple-element.717) | copy-start | bytes 393220
  207.6 12.7 %copy-start.22 = (bf16[1,2,128]{2,1,0:T(2,128)(2,1)S(1)}, bf16[1,2,128]{2,1,0:T(2,128)(2,1)}, u32[]{:S(2)}) copy-start(bf16[1,2,128]{2,1,0:T(2,128)(2,1)} %get-tuple-element.720) | copy-start | bytes 1540
  207.6 17.8 %copy-start.1 = (f32[2,128,256]{2,1,0:T(8,128)S(1)}, f32[2,128,256]{2,1,0:T(8,128)}, u32[]{:S(2)}) copy-start(f32[2,128,256]{2,1,0:T(8,128)} %custom-call.2) | copy-start | bytes 786436
  207.6 17.8 %copy-start.18 = (f32[2,128]{1,0:T(2,128)S(1)}, f32[2,128]{1,0:T(2,128)}, u32[]{:S(2)}) copy-start(f32[2,128]{1,0:T(2,128)} %custom-call.1) | copy-start | bytes 3076
  212.4 17.3 %copy-start.13 = (f32[128,256]{1,0:T(8,128)S(1)}, f32[128,256]{1,0:T(8,128)}, u32[]{:S(2)}) copy-start(f32[128,256]{1,0:T(8,128)} %broadcast_multiply_fusion) | copy-start | bytes 393220
  212.4 18.1 %copy-start.12 = (f32[2,64,2,128]{3,2,1,0:T(2,128)S(1)}, f32[2,64,2,128]{3,2,1,0:T(2,128)}, u32[]{:S(2)}) copy-start(f32[2,64,2,128]{3,2,1,0:T(2,128)} %reshape.134) | copy-start | bytes 393220
  225.4 6.9 %copy-start.2 = (f32[2,64,2,256]{3,2,1,0:T(2,128)S(1)}, f32[2,64,2,256]{3,2,1,0:T(2,128)}, u32[]{:S(2)}) copy-start(f32[2,64,2,256]{3,2,1,0:T(2,128)} %reshape_reshape.7) | copy-start | bytes 786436
  241.4 4.1 %copy-start.20 = (f32[512]{0:T(512)S(1)}, f32[512]{0:T(512)}, u32[]{:S(2)}) copy-start(f32[512]{0:T(512)} %param.44) | copy-start | bytes 6148
  241.4 4.9 %copy-start.24 = (f32[2,512]{1,0:T(2,128)S(1)}, f32[2,512]{1,0:T(2,128)}, u32[]{:S(2)}) copy-start(f32[2,512]{1,0:T(2,128)} %get-tuple-element.705) | copy-start | bytes 12292
  241.4 42.4 %copy-start.6 = (bf16[128,512]{1,0:T(8,128)(2,1)S(1)}, bf16[128,512]{1,0:T(8,128)(2,1)}, u32[]{:S(2)}) copy-start(bf16[128,512]{1,0:T(8,128)(2,1)} %param.29) | copy-start | bytes 393220
Sparse Core Ops, SparseCore 0:
  48.0 36.1 all-gather.6
  246.4 37.3 all-gather.8
